TPU v7x, 32 devices: a whole 2x2x4 slice. The times are simulated.
32 devices in a mesh: ep: 8 (over z, y), tp: 4 (over x, core).
Axes of the slice: x: 2, y: 2, z: 4, core: 2. Of those that a mesh axis runs over, the one named last changes fastest.
Arguments:
- tokens_a: bfloat16 [1024, 2048], P('ep'), may hold values from -30 to 30
- attn_gain: float32 [2048], replicated, may hold values from 0.1 to 1.9
- w_query: bfloat16 [2048, 2048], P(None, 'tp'), may hold values from -2 to 2
- w_query_rot: bfloat16 [2048, 1024], P(None, 'tp'), may hold values from -0.125 to 0.125
- w_latent: bfloat16 [2048, 512], replicated, may hold values from -2 to 2
- w_key_rot: bfloat16 [2048, 32], replicated, may hold values from -0.125 to 0.125
- latent_gain: float32 [512], replicated, may hold values from 0.1 to 1.9
- w_key_up: bfloat16 [512, 2048], P(None, 'tp'), may hold values from -2 to 2
- w_value_up: bfloat16 [512, 2048], P(None, 'tp'), may hold values from -0.25 to 0.25
- w_output: bfloat16 [2048, 2048], P('tp'), may hold values from -0.125 to 0.125
- tokens_b: bfloat16 [2048, 2048], P('ep'), may hold values from -6 to 6
- ffn_gain: float32 [2048], replicated, may hold values from 0.1 to 1.9
- expert_ids: int32 [2048, 2], P('ep'), may hold values from 0 to 7, all different within a row; in each aligned block of 256 rows (0 to 255, 256 to 511, ...) at most 128 rows name the same one
- expert_weights: float32 [2048, 2], P('ep'), may hold values from 0.1 to 1
- w_gate: bfloat16 [8, 2048, 1024], P('ep', None, 'tp'), may hold values from -0.125 to 0.125
- w_up: bfloat16 [8, 2048, 1024], P('ep', None, 'tp'), may hold values from -0.125 to 0.125
- w_down: bfloat16 [8, 1024, 2048], P('ep', 'tp'), may hold values from -0.1875 to 0.1875
Outputs:
- mixed_a: bfloat16 [1024, 2048], P(('ep', 'tp'))
- mixed_b: bfloat16 [2048, 2048], P('ep', 'tp')
Inputs may be any that keep to these rules, and one draw needn't show every extreme that they name: `expert_ids`: each row names 2 different experts. In the 256 rows of one index of ep no expert is named more than 128 times, and in some such block one expert is named exactly 128 times.
All inputs are finite; a program needn't handle non-finite values.
Results may differ from a plain program's by a relative error of at most 0.012.
Values may be sent and summed in bfloat16 or wider, within the bound.
A program may use at most 192 MiB of HBM per device.

v0:
```python
import jax
import jax.numpy as jnp
from jax import lax
from jax.sharding import PartitionSpec as P

NOPE = 64
ROPE = 32
VD = 64


epsilon = 1e-06
rope_base = 10000.0


def normalize(matrix, gain):
    floats = matrix.astype(jnp.float32)
    scaled = floats * lax.rsqrt(jnp.mean(floats * floats, axis=-1, keepdims=True) + epsilon)
    return scaled * gain


def rotate(vectors, positions):
    rot_width = vectors.shape[-1]
    half_width = rot_width // 2
    inverse = rope_base ** (-(jnp.arange(half_width, dtype=jnp.float32) * 2.0) / rot_width)
    angles = positions.astype(jnp.float32)[:, None] * inverse[None, :]
    cosine = jnp.cos(angles)[:, None, :]
    sine_part = jnp.sin(angles)[:, None, :]
    first_half = vectors[..., :half_width]
    second_half = vectors[..., half_width:]
    return jnp.concatenate(
        [
            first_half * cosine - second_half * sine_part,
            first_half * sine_part + second_half * cosine,
        ],
        axis=-1,
    )


def attention_half(
    tokens_a,
    attn_gain,
    w_query,
    w_query_rot,
    w_latent,
    w_key_rot,
    latent_gain,
    w_key_up,
    w_value_up,
    w_output,
):
    row_count = tokens_a.shape[0]
    head_count = w_query.shape[1] // NOPE
    offset = lax.axis_index("ep") * row_count
    positions = offset + jnp.arange(row_count, dtype=jnp.int32)
    normed = normalize(tokens_a, attn_gain).astype(jnp.bfloat16)
    query_plain = jnp.dot(normed, w_query, preferred_element_type=jnp.float32).astype(jnp.bfloat16)
    query_plain = query_plain.reshape(row_count, head_count, NOPE)
    turned = jnp.dot(normed, w_query_rot, preferred_element_type=jnp.float32).reshape(
        row_count, head_count, ROPE
    )
    query_rotated_rows = rotate(turned, positions).astype(jnp.bfloat16)
    latent = normalize(
        jnp.dot(normed, w_latent, preferred_element_type=jnp.float32), latent_gain
    ).astype(jnp.bfloat16)
    key_raw = jnp.dot(normed, w_key_rot, preferred_element_type=jnp.float32)[:, None, :]
    key_turned = rotate(key_raw, positions)[:, 0, :].astype(jnp.bfloat16)
    logit_scale = (NOPE + ROPE) ** (-0.5)
    pieces = (
        lax.all_gather(latent, "ep", axis=0, tiled=True),
        lax.all_gather(key_turned, "ep", axis=0, tiled=True),
    )
    piece_keys = jnp.dot(pieces[0], w_key_up, preferred_element_type=jnp.float32).astype(
        jnp.bfloat16
    )
    piece_values = jnp.dot(pieces[0], w_value_up, preferred_element_type=jnp.float32).astype(
        jnp.bfloat16
    )
    key_count = piece_keys.shape[0]
    blocks = key_count // row_count
    key_blocks = piece_keys.reshape(blocks, row_count, head_count, NOPE)
    value_blocks = piece_values.reshape(blocks, row_count, head_count, VD)
    rotated_key_blocks = pieces[1].reshape(blocks, row_count, ROPE)
    score_matrix = (
        jnp.einsum("yvz,wrvz->yvwr", query_plain, key_blocks, preferred_element_type=jnp.float32)
        + jnp.einsum(
            "yjx,inx->yjin",
            query_rotated_rows,
            rotated_key_blocks,
            preferred_element_type=jnp.float32,
        )
    ) * logit_scale
    key_pos = jnp.arange(key_count, dtype=jnp.int32).reshape(blocks, row_count)
    allowed = key_pos[None, None, :, :] <= positions[:, None, None, None]
    masked = jnp.where(allowed, score_matrix, -1e30)
    block_max = jnp.max(masked, axis=-1)
    probs = jnp.where(allowed, jnp.exp(masked - block_max[..., None]), 0.0)
    block_total = jnp.sum(probs, axis=-1)
    block_out = jnp.einsum(
        "qhbk,bkhd->qhbd",
        probs.astype(jnp.bfloat16),
        value_blocks,
        preferred_element_type=jnp.float32,
    )
    run_max = jnp.full((row_count, head_count), -1e30, jnp.float32)
    new_max = jnp.maximum(run_max, jnp.max(block_max, axis=-1))
    new_factor = jnp.exp(block_max - new_max[..., None])
    new_total = jnp.sum(new_factor * block_total, axis=-1)
    new_out = jnp.sum(new_factor[..., None] * block_out, axis=2)
    attended = (
        (new_out / new_total[..., None]).astype(jnp.bfloat16).reshape(row_count, head_count * VD)
    )
    return lax.psum_scatter(
        jnp.dot(attended, w_output, preferred_element_type=jnp.float32).astype(jnp.bfloat16),
        "tp",
        scatter_dimension=0,
        tiled=True,
    )


def expert_half(tokens_b, ffn_gain, expert_ids, expert_weights, w_gate, w_up, w_down):
    row_count = tokens_b.shape[0]
    top_count = expert_ids.shape[1]
    expert_count = w_gate.shape[0] * lax.axis_size("ep")
    capacity = 2 * row_count * top_count // expert_count
    normed = normalize(tokens_b, ffn_gain).astype(jnp.bfloat16)
    flat_ids = expert_ids.reshape(-1)
    pair_count = flat_ids.shape[0]
    onehot = (flat_ids[:, None] == jnp.arange(expert_count, dtype=jnp.int32)[None, :]).astype(
        jnp.int32
    )
    before = jnp.cumsum(onehot, axis=0) - onehot
    slot_index = jnp.sum(before * onehot, axis=1)
    target = flat_ids * capacity + slot_index
    source_row = (
        jnp.zeros((expert_count * capacity,), jnp.int32)
        .at[target]
        .set(jnp.arange(pair_count, dtype=jnp.int32) // top_count)
    )
    occupied = jnp.zeros((expert_count * capacity,), jnp.int32).at[target].set(1)
    outgoing = jnp.where(occupied[:, None] > 0, normed[source_row], jnp.zeros((), jnp.bfloat16))
    outgoing = outgoing.reshape(expert_count, capacity, normed.shape[1])
    gate_weight = w_gate[0]
    up_weight = w_up[0]
    down_weight = w_down[0]
    arrived = lax.all_to_all(outgoing, "ep", split_axis=0, concat_axis=0, tiled=True)
    flat_rows = arrived.reshape(-1, arrived.shape[-1])
    gate_part = jnp.dot(flat_rows, gate_weight, preferred_element_type=jnp.float32)
    up_part = jnp.dot(flat_rows, up_weight, preferred_element_type=jnp.float32)
    hidden_rows = (jax.nn.silu(gate_part) * up_part).astype(jnp.bfloat16)
    hidden = hidden_rows.reshape(arrived.shape[0], arrived.shape[1], gate_weight.shape[1])
    partial_value = jnp.dot(
        hidden.reshape(-1, hidden.shape[-1]), down_weight, preferred_element_type=jnp.float32
    )
    partial_value = partial_value.reshape(expert_count, capacity, down_weight.shape[1])
    summed = lax.psum_scatter(
        partial_value.astype(jnp.bfloat16), "tp", scatter_dimension=2, tiled=True
    )
    returned = lax.all_to_all(summed, "ep", split_axis=0, concat_axis=0, tiled=True)
    picked = returned.reshape(expert_count * capacity, -1)[target].astype(jnp.float32)
    picked = picked.reshape(row_count, top_count, -1)
    shares = expert_weights / jnp.sum(expert_weights, axis=1, keepdims=True)
    return jnp.sum(picked * shares[:, :, None], axis=1).astype(jnp.bfloat16)


def on_device(
    tokens_a,
    attn_gain,
    w_query,
    w_query_rot,
    w_latent,
    w_key_rot,
    latent_gain,
    w_key_up,
    w_value_up,
    w_output,
    tokens_b,
    ffn_gain,
    expert_ids,
    expert_weights,
    w_gate,
    w_up,
    w_down,
):
    mixed_a = attention_half(
        tokens_a,
        attn_gain,
        w_query,
        w_query_rot,
        w_latent,
        w_key_rot,
        latent_gain,
        w_key_up,
        w_value_up,
        w_output,
    )
    mixed_b = expert_half(tokens_b, ffn_gain, expert_ids, expert_weights, w_gate, w_up, w_down)
    return (mixed_a, mixed_b)


def solution(mesh):
    placed = (
        P("ep", None),
        P(),
        P(None, "tp"),
        P(None, "tp"),
        P(),
        P(),
        P(),
        P(None, "tp"),
        P(None, "tp"),
        P("tp", None),
        P("ep", None),
        P(),
        P("ep", None),
        P("ep", None),
        P("ep", None, "tp"),
        P("ep", None, "tp"),
        P("ep", "tp", None),
    )
    return jax.shard_map(
        on_device,
        mesh=mesh,
        in_specs=placed,
        out_specs=(P(("ep", "tp"), None), P("ep", "tp")),
        check_vma=False,
    )
```

profile of v0, /device:TPU:0, one launch (start us, length us, event | category | flops | bytes accessed | tf_op | source)
XLA Modules:
  0.0 242.8 jit_solution(2341269000058259114)
XLA Ops:
  11.8 2.4 %scatter_custom_fusion.1 = s32[1024]{0:T(1024)S(1)} fusion(s32[512]{0:T(512)S(1)} %bitcast.84, s32[512]{0:T(512)S(1)} %add_select_fusion, s32[]{:T(128)} %constant.64.clone.1), kind=kCustom, calls=%fused_computation.88 | custom fusion | bytes 4100 | tf_op jit(solution)/shard_map/scatter | solution.py:137
  15.8 2.4 %scatter_custom_fusion = s32[1024]{0:T(1024)S(1)} fusion(s32[512]{0:T(512)S(1)} %bitcast.85, s32[512]{0:T(512)S(1)} %broadcast.240, s32[]{:T(128)} %constant.64.clone.1), kind=kCustom, calls=%fused_computation.90 | custom fusion | bytes 4100 | tf_op jit(solution)/shard_map/scatter | solution.py:139
  19.8 6.0 %gather_fusion = bf16[1024,2048]{1,0:T(8,128)(2,1)} fusion(bf16[256,2048]{1,0:T(8,128)(2,1)S(1)} %fusion.6, s32[1024]{0:T(1024)S(1)} %fusion.43), kind=kCustom, calls=%fused_computation | custom fusion | bytes 8392704 | tf_op jit(solution)/shard_map/gather | solution.py:140
  25.8 4.5 %broadcast_select_fusion = bf16[8,128,2048]{2,1,0:T(8,128)(2,1)} fusion(bf16[8,128,2048]{2,1,0:T(8,128)(2,1)} %bitcast.77, pred[8,128]{1,0:T(8,128)(4,1)S(1)} %compare_bitcast_fusion), kind=kLoop, calls=%fused_computation.8 | loop fusion | flops 2097152 | bytes 8389632 | tf_op jit(solution)/shard_map/jit(_where)/select_n | solution.py:140
  30.3 7.4 %all-to-all-start = ((bf16[8,128,2048]{2,1,0:T(8,128)(2,1)}), bf16[8,128,2048]{2,1,0:T(8,128)(2,1)}, u32[]{:S(2)}, u32[]{:S(2)}) async-start(bf16[8,128,2048]{2,1,0:T(8,128)(2,1)} %broadcast_select_fusion), calls=%async_computation.1 | async-start | bytes 8388608 | tf_op jit(solution)/shard_map/all_to_all | solution.py:145
  38.0 2.2 multiply_reduce_fusion.1
  41.0 102.7 %all-to-all-done = bf16[8,128,2048]{2,1,0:T(8,128)(2,1)} async-done(((bf16[8,128,2048]{2,1,0:T(8,128)(2,1)}), bf16[8,128,2048]{2,1,0:T(8,128)(2,1)}, u32[]{:S(2)}, u32[]{:S(2)}) %all-to-all-start) | async-done | bytes 4194336 | tf_op jit(solution)/shard_map/all_to_all | solution.py:145
  143.6 3.8 %fusion.22 = f32[1024,256]{1,0:T(8,128)S(1)} fusion(bf16[1024,2048]{1,0:T(8,128)(2,1)} %bitcast.17, bf16[1,2048,256]{2,1,0:T(8,128)(2,1)} %param.31), kind=kOutput, calls=%fused_computation.40 | convolution fusion | flops 1073741824 | bytes 6291456 | tf_op jit(solution)/shard_map/dot_general | solution.py:147
  147.5 3.6 %fusion.16 = bf16[1024,256]{1,0:T(8,128)(2,1)S(1)} fusion(bf16[1024,2048]{1,0:T(8,128)(2,1)} %bitcast.17, bf16[1,2048,256]{2,1,0:T(8,128)(2,1)S(1)} %copy-done.6, f32[1024,256]{1,0:T(8,128)S(1)} %fusion.22), kind=kOutput, calls=%fused_computation.32 | convolution fusion | flops 1075314688 | bytes 6815744 | tf_op jit(solution)/shard_map/dot_general | solution.py:148
  151.1 3.2 %convolution_convert_fusion = bf16[8,128,2048]{2,1,0:T(8,128)(2,1)} fusion(bf16[8,128,256]{2,1,0:T(8,128)(2,1)S(1)} %bitcast.79, bf16[1,256,2048]{2,1,0:T(8,128)(2,1)S(1)} %copy-done.2), kind=kOutput, calls=%fused_computation.9 | convolution fusion | flops 1075838976 | bytes 5767168 | tf_op jit(solution)/shard_map/dot_general | solution.py:151
  154.8 26.2 %all-gather = bf16[1024,1,32]{0,2,1:T(8,128)(2,1)S(1)} all-gather(bf16[128,1,32]{0,2,1:T(8,128)(2,1)S(1)} %pad_maximum_fusion), channel_id=2, replica_groups=mesh['ep'=8,'tp'=4] {'ep'}, dimensions={0}, use_global_device_ids=true | all-gather | bytes 73728 | tf_op jit(solution)/shard_map/all_gather | solution.py:70
  181.1 2.1 convolution_convert_fusion.4
  183.6 1.8 fusion.55
  185.5 2.1 convolution_convert_fusion.3
  187.6 2.1 reshape.303
  189.7 2.1 convolution_convert_fusion.2
  191.8 2.1 reshape.304
  193.8 2.3 fusion.11
  197.2 2.0 copy-done.1
  200.4 3.6 %all-to-all-start.1 = ((bf16[8,128,512]{2,1,0:T(8,128)(2,1)}), bf16[8,128,512]{2,1,0:T(8,128)(2,1)S(1)}, u32[]{:S(2)}, u32[]{:S(2)}) async-start(bf16[8,128,512]{2,1,0:T(8,128)(2,1)} %reduce-scatter.5.cloned.1.call-done), calls=%async_computation.3 | async-start | bytes 2097152 | tf_op jit(solution)/shard_map/all_to_all | solution.py:158
  204.0 4.0 %fusion.9 = f32[128,8,64]{0,2,1:T(8,128)S(1)} fusion(f32[128,8,8]{0,2,1:T(8,128)S(1)} %get-tuple-element.5, f32[128,8,8,128]{0,3,2,1:T(8,128)} %copy-done.1, f32[128,8,8]{0,2,1:T(8,128)S(1)} %get-tuple-element.14, pred[128,8,128]{0,2,1:T(8,128)(4,1)S(1)} %broadcast_compare_fusion, bf16[8,128,8,64]{3,2,1,0:T(8,128)(2,1)} %reshape.304), kind=kOutput, calls=%fused_computation.20 | convolution fusion | flops 138346496 | bytes 5701632 | tf_op jit(solution)/shard_map/qhbk,bkhd->qhbd/dot_general | solution.py:98
  209.5 19.4 %all-to-all-done.1 = bf16[8,128,512]{2,1,0:T(8,128)(2,1)S(1)} async-done(((bf16[8,128,512]{2,1,0:T(8,128)(2,1)}), bf16[8,128,512]{2,1,0:T(8,128)(2,1)S(1)}, u32[]{:S(2)}, u32[]{:S(2)}) %all-to-all-start.1) | async-done | bytes 1048608 | tf_op jit(solution)/shard_map/all_to_all | solution.py:158
  229.0 2.6 %gather_fusion.1 = bf16[512,512]{1,0:T(8,128)(2,1)} fusion(bf16[1024,512]{1,0:T(8,128)(2,1)S(1)} %bitcast.76, s32[1024]{0:T(1024)S(1)} %pad_clamp_fusion), kind=kCustom, calls=%fused_computation.1 | custom fusion | bytes 1050624 | tf_op jit(solution)/shard_map/gather | solution.py:159
  233.3 2.1 multiply_reduce_fusion
  (73 shorter events, 14.4 us)
Async XLA Ops:
  8.0 200.0 %copy-start = (bf16[512,2048]{1,0:T(8,128)(2,1)S(1)}, bf16[512,2048]{1,0:T(8,128)(2,1)}, u32[]{:S(2)}) copy-start(bf16[512,2048]{1,0:T(8,128)(2,1)} %param.26) | copy-start | bytes 6291460
  30.3 7.5 %copy-start.3 = (bf16[128,2048]{1,0:T(8,128)(2,1)S(1)}, bf16[128,2048]{1,0:T(8,128)(2,1)}, u32[]{:S(2)}) copy-start(bf16[128,2048]{1,0:T(8,128)(2,1)} %param.17) | copy-start | bytes 1572868
  30.3 7.7 %copy-start.8 = (f32[2048]{0:T(1024)S(1)}, f32[2048]{0:T(1024)}, u32[]{:S(2)}) copy-start(f32[2048]{0:T(1024)} %param.18) | copy-start | bytes 24580
  30.3 9.9 %copy-start.5 = (f32[512]{0:T(512)S(1)}, f32[512]{0:T(512)}, u32[]{:S(2)}) copy-start(f32[512]{0:T(512)} %param.23) | copy-start | bytes 6148
  30.3 113.4 %all-to-all-start = ((bf16[8,128,2048]{2,1,0:T(8,128)(2,1)}), bf16[8,128,2048]{2,1,0:T(8,128)(2,1)}, u32[]{:S(2)}, u32[]{:S(2)}) async-start(bf16[8,128,2048]{2,1,0:T(8,128)(2,1)} %broadcast_select_fusion), calls=%async_computation.1 | async-start | bytes 8388608 | tf_op jit(solution)/shard_map/all_to_all | solution.py:145
  37.7 147.8 %all-gather.3.cloned.1.call-start = ((), (), s32[]{:S(2)}) async-start(), calls=%async_computation.4 | async-start | bytes 1179648 | tf_op jit(solution)/shard_map/all_gather | solution.py:69
  40.9 159.5 %reduce-scatter.5.cloned.1.call-start = ((), (), s32[]{:S(2)}) async-start(), calls=%async_computation.6 | async-start | bytes 5242880 | tf_op jit(solution)/shard_map/reduce_scatter | solution.py:155
  143.6 3.8 %copy-start.6 = (bf16[1,2048,256]{2,1,0:T(8,128)(2,1)S(1)}, bf16[1,2048,256]{2,1,0:T(8,128)(2,1)}, u32[]{:S(2)}) copy-start(bf16[1,2048,256]{2,1,0:T(8,128)(2,1)} %param.32) | copy-start | bytes 3145732
  147.5 3.6 %copy-start.2 = (bf16[1,256,2048]{2,1,0:T(8,128)(2,1)S(1)}, bf16[1,256,2048]{2,1,0:T(8,128)(2,1)}, u32[]{:S(2)}) copy-start(bf16[1,256,2048]{2,1,0:T(8,128)(2,1)} %param.33) | copy-start | bytes 3145732
  151.1 3.3 %copy-start.7 = (bf16[2048,32]{0,1:T(8,128)(2,1)S(1)}, bf16[2048,32]{0,1:T(8,128)(2,1)}, u32[]{:S(2)}) copy-start(bf16[2048,32]{0,1:T(8,128)(2,1)} %param.22) | copy-start | bytes 393220
  197.2 2.0 copy-start.1
  200.4 28.6 %all-to-all-start.1 = ((bf16[8,128,512]{2,1,0:T(8,128)(2,1)}), bf16[8,128,512]{2,1,0:T(8,128)(2,1)S(1)}, u32[]{:S(2)}, u32[]{:S(2)}) async-start(bf16[8,128,512]{2,1,0:T(8,128)(2,1)} %reduce-scatter.5.cloned.1.call-done), calls=%async_computation.3 | async-start | bytes 2097152 | tf_op jit(solution)/shard_map/all_to_all | solution.py:158
  204.0 31.4 %reduce-scatter.3.cloned.1.call-start = ((), (), s32[]{:S(2)}) async-start(), calls=%async_computation.5 | async-start | bytes 655360 | tf_op jit(solution)/shard_map/reduce_scatter | solution.py:112
  204.0 5.3 %copy-start.4 = (f32[256,2]{0,1:T(2,128)S(1)}, f32[256,2]{0,1:T(2,128)}, u32[]{:S(2)}) copy-start(f32[256,2]{0,1:T(2,128)} %param.30) | copy-start | bytes 6148
Sparse Core Ops, SparseCore 0:
  41.2 102.9 all-gather.2
Sparse Core Ops, SparseCore 1:
  154.4 43.3 reduce-scatter.4
  209.4 22.8 reduce-scatter.2
where the time goes:
time: 243 us
  waiting for transfers between devices  122 us (50%)
  matrix products  29.6 us (12%)
  blocking collectives  26.2 us (11%)
  local copies, waits for them, and re-layouts  23.5 us (10%)
  between operations  15.9 us (7%)
  other arithmetic  14.3 us (6%)
  starting transfers between devices  11.1 us (5%)
    all_to_all x1, waiting for transfers between devices, expert_half(): lax.all_to_all(outgoing, 'ep', split_axis=0, concat_axis=0, tiled=True)  103 us
    all_gather x1, blocking collectives, attention_half(): lax.all_gather(key_turned, 'ep', axis=0, tiled=True)  26.2 us
    all_to_all x1, waiting for transfers between devices, expert_half(): lax.all_to_all(summed, 'ep', split_axis=0, concat_axis=0, tiled=True)  19.4 us
    all_to_all x1, starting transfers between devices, expert_half(): lax.all_to_all(outgoing, 'ep', split_axis=0, concat_axis=0, tiled=True)  7.44 us
    gather x1, local copies, waits for them, and re-layouts, expert_half(): normed[source_row]  6.03 us
  transfers between devices with their start and end apart: 5, of which 2 were waited for; matrix products, arithmetic and copies ran while one was open for 18% of the time, Pallas kernels for 0%

commit v1 on v0

--- a/solution.py
+++ b/solution.py
@@ -47,6 +47,7 @@
     w_key_up,
     w_value_up,
     w_output,
+    outgoing,
 ):
     row_count = tokens_a.shape[0]
     head_count = w_query.shape[1] // NOPE
@@ -65,10 +66,13 @@
     key_raw = jnp.dot(normed, w_key_rot, preferred_element_type=jnp.float32)[:, None, :]
     key_turned = rotate(key_raw, positions)[:, 0, :].astype(jnp.bfloat16)
     logit_scale = (NOPE + ROPE) ** (-0.5)
-    pieces = (
-        lax.all_gather(latent, "ep", axis=0, tiled=True),
-        lax.all_gather(key_turned, "ep", axis=0, tiled=True),
-    )
+    outgoing, compact = lax.optimization_barrier(
+        (outgoing, jnp.concatenate([latent, key_turned], axis=1))
+    )
+    joined = lax.all_gather(compact, "ep", axis=0, tiled=True)
+    arrived = lax.all_to_all(outgoing, "ep", split_axis=0, concat_axis=0, tiled=True)
+    joined, arrived = lax.optimization_barrier((joined, arrived))
+    pieces = (joined[:, : latent.shape[1]], joined[:, latent.shape[1] :])
     piece_keys = jnp.dot(pieces[0], w_key_up, preferred_element_type=jnp.float32).astype(
         jnp.bfloat16
     )
@@ -109,57 +113,101 @@
     attended = (
         (new_out / new_total[..., None]).astype(jnp.bfloat16).reshape(row_count, head_count * VD)
     )
-    return lax.psum_scatter(
+    mixed = lax.psum_scatter(
         jnp.dot(attended, w_output, preferred_element_type=jnp.float32).astype(jnp.bfloat16),
         "tp",
         scatter_dimension=0,
         tiled=True,
     )
-
-
-def expert_half(tokens_b, ffn_gain, expert_ids, expert_weights, w_gate, w_up, w_down):
-    row_count = tokens_b.shape[0]
+    return mixed, arrived
+
+
+def dispatch_rows(tokens_b, ffn_gain, expert_ids, expert_count):
+    row_count, width = tokens_b.shape
     top_count = expert_ids.shape[1]
-    expert_count = w_gate.shape[0] * lax.axis_size("ep")
     capacity = 2 * row_count * top_count // expert_count
-    normed = normalize(tokens_b, ffn_gain).astype(jnp.bfloat16)
-    flat_ids = expert_ids.reshape(-1)
-    pair_count = flat_ids.shape[0]
-    onehot = (flat_ids[:, None] == jnp.arange(expert_count, dtype=jnp.int32)[None, :]).astype(
-        jnp.int32
-    )
-    before = jnp.cumsum(onehot, axis=0) - onehot
-    slot_index = jnp.sum(before * onehot, axis=1)
-    target = flat_ids * capacity + slot_index
-    source_row = (
-        jnp.zeros((expert_count * capacity,), jnp.int32)
-        .at[target]
-        .set(jnp.arange(pair_count, dtype=jnp.int32) // top_count)
-    )
-    occupied = jnp.zeros((expert_count * capacity,), jnp.int32).at[target].set(1)
-    outgoing = jnp.where(occupied[:, None] > 0, normed[source_row], jnp.zeros((), jnp.bfloat16))
-    outgoing = outgoing.reshape(expert_count, capacity, normed.shape[1])
-    gate_weight = w_gate[0]
-    up_weight = w_up[0]
-    down_weight = w_down[0]
-    arrived = lax.all_to_all(outgoing, "ep", split_axis=0, concat_axis=0, tiled=True)
-    flat_rows = arrived.reshape(-1, arrived.shape[-1])
-    gate_part = jnp.dot(flat_rows, gate_weight, preferred_element_type=jnp.float32)
-    up_part = jnp.dot(flat_rows, up_weight, preferred_element_type=jnp.float32)
-    hidden_rows = (jax.nn.silu(gate_part) * up_part).astype(jnp.bfloat16)
-    hidden = hidden_rows.reshape(arrived.shape[0], arrived.shape[1], gate_weight.shape[1])
-    partial_value = jnp.dot(
-        hidden.reshape(-1, hidden.shape[-1]), down_weight, preferred_element_type=jnp.float32
-    )
-    partial_value = partial_value.reshape(expert_count, capacity, down_weight.shape[1])
-    summed = lax.psum_scatter(
-        partial_value.astype(jnp.bfloat16), "tp", scatter_dimension=2, tiled=True
-    )
-    returned = lax.all_to_all(summed, "ep", split_axis=0, concat_axis=0, tiled=True)
-    picked = returned.reshape(expert_count * capacity, -1)[target].astype(jnp.float32)
-    picked = picked.reshape(row_count, top_count, -1)
+    tp_count = lax.axis_size("tp")
+    part_width = width // tp_count
+    floats = tokens_b.astype(jnp.float32)
+    factor = lax.rsqrt(jnp.mean(floats * floats, axis=-1, keepdims=True) + epsilon)
+    start = lax.axis_index("tp") * part_width
+    own = lax.dynamic_slice_in_dim(tokens_b, start, part_width, 1).astype(jnp.float32)
+    own_gain = lax.dynamic_slice_in_dim(ffn_gain, start, part_width, 0)
+    normed = (own * factor * own_gain).astype(jnp.bfloat16)
+    experts = jnp.arange(expert_count, dtype=jnp.int32)
+    slots = jnp.arange(capacity, dtype=jnp.int32)
+    named = (expert_ids[:, :, None] == experts).any(axis=1)
+    rows = jnp.arange(row_count, dtype=jnp.int32)
+    earlier = (rows[:, None] > rows[None, :]).astype(jnp.bfloat16)
+    before = jnp.dot(
+        earlier, named.astype(jnp.bfloat16), preferred_element_type=jnp.float32
+    ).astype(jnp.int32)
+    slot_of = jnp.where(named, before, -1).T
+    chosen = (slot_of[:, None, :] == slots[None, :, None]).astype(jnp.bfloat16)
+    outgoing = jnp.dot(
+        chosen.reshape(expert_count * capacity, row_count),
+        normed,
+        preferred_element_type=jnp.float32,
+    ).astype(jnp.bfloat16)
+    outgoing = outgoing.reshape(expert_count, capacity, part_width)
+    return outgoing, before
+
+
+def swap(block, distance, count):
+    return lax.ppermute(block, "tp", [(i, i ^ distance) for i in range(count)])
+
+
+def expert_half(arrived, before, expert_ids, expert_weights, w_gate, w_up, w_down):
+    expert_count, capacity, part_width = arrived.shape
+    tp_count = lax.axis_size("tp")
+    top_count = expert_ids.shape[1]
+    experts = jnp.arange(expert_count, dtype=jnp.int32)
+    me = lax.axis_index("tp")
+    blocks = {0: arrived.reshape(-1, part_width)}
+    distance = tp_count // 2
+    while distance:
+        for mask in list(blocks):
+            blocks[mask ^ distance] = swap(blocks[mask], distance, tp_count)
+        distance //= 2
+    gate_part = 0.0
+    up_part = 0.0
+    for mask, block in blocks.items():
+        first = (me ^ mask) * part_width
+        gate_rows = lax.dynamic_slice_in_dim(w_gate[0], first, part_width, 0)
+        up_rows = lax.dynamic_slice_in_dim(w_up[0], first, part_width, 0)
+        gate_part += jnp.dot(block, gate_rows, preferred_element_type=jnp.float32)
+        up_part += jnp.dot(block, up_rows, preferred_element_type=jnp.float32)
+    hidden = (jax.nn.silu(gate_part) * up_part).astype(jnp.bfloat16)
+    parts = {}
+    for mask in reversed(range(tp_count)):
+        down_columns = lax.dynamic_slice_in_dim(w_down[0], (me ^ mask) * part_width, part_width, 1)
+        parts[mask] = jnp.dot(hidden, down_columns, preferred_element_type=jnp.float32)
+    distance = 1
+    while distance < tp_count:
+        for mask in [m for m in parts if m & distance]:
+            came = swap(parts.pop(mask).astype(jnp.bfloat16), distance, tp_count)
+            parts[mask ^ distance] += came.astype(jnp.float32)
+        distance *= 2
+    summed = parts[0].astype(jnp.bfloat16)
+    returned = lax.all_to_all(
+        summed.reshape(expert_count, capacity, part_width),
+        "ep",
+        split_axis=0,
+        concat_axis=0,
+        tiled=True,
+    )
     shares = expert_weights / jnp.sum(expert_weights, axis=1, keepdims=True)
-    return jnp.sum(picked * shares[:, :, None], axis=1).astype(jnp.bfloat16)
+    table = returned.reshape(expert_count * capacity, part_width)
+    total = 0.0
+    for k in range(top_count):
+        own_slot = jnp.sum(jnp.where(expert_ids[:, k : k + 1] == experts, before, 0), axis=1)
+        target = expert_ids[:, k] * capacity + own_slot
+        pick = (
+            target[:, None] == jnp.arange(expert_count * capacity, dtype=jnp.int32)
+        ).astype(jnp.bfloat16)
+        picked = jnp.dot(pick, table, preferred_element_type=jnp.float32)
+        total = total + picked * shares[:, k : k + 1]
+    return total.astype(jnp.bfloat16)
 
 
 def on_device(
@@ -181,7 +229,9 @@
     w_up,
     w_down,
 ):
-    mixed_a = attention_half(
+    expert_count = w_gate.shape[0] * lax.axis_size("ep")
+    outgoing, before = dispatch_rows(tokens_b, ffn_gain, expert_ids, expert_count)
+    mixed_a, arrived = attention_half(
         tokens_a,
         attn_gain,
         w_query,
@@ -192,8 +242,9 @@
         w_key_up,
         w_value_up,
         w_output,
-    )
-    mixed_b = expert_half(tokens_b, ffn_gain, expert_ids, expert_weights, w_gate, w_up, w_down)
+        outgoing,
+    )
+    mixed_b = expert_half(arrived, before, expert_ids, expert_weights, w_gate, w_up, w_down)
     return (mixed_a, mixed_b)
 
 

time: 243 us -> 180 us (0.74)
  waiting for transfers between devices: 122 us -> 88 us
  blocking collectives: 26.2 us -> 0 us
  local copies, waits for them, and re-layouts: 23.5 us -> 10.7 us
  matrix products: 29.6 us -> 40 us
  starting transfers between devices: 11.1 us -> 15 us
  other arithmetic: 14.3 us -> 11.3 us
    all_to_all x2, waiting for transfers between devices: 122 us -> 47.3 us  [the longest x1 27.4 us: attention_half(): lax.all_to_all(outgoing, 'ep', split_axis=0, concat_axis=0, tiled=True)]
    ppermute x0 -> x6, waiting for transfers between devices: none -> 27.3 us  [swap(): return lax.ppermute(block, 'tp', [(i, i ^ distance) for i in range(count)])]
    all_gather x1 -> x0, blocking collectives: 26.2 us -> none  [attention_half(): lax.all_gather(key_turned, 'ep', axis=0, tiled=True)]
    all_gather x1, waiting for transfers between devices: 0.02 us -> 12.1 us  [attention_half(): joined = lax.all_gather(compact, 'ep', axis=0, tiled=True)]
    gather x2 -> x0, local copies, waits for them, and re-layouts: 8.65 us -> none  [the longest x1 6.03 us: expert_half(): normed[source_row]]
    dot_general x3 -> x16, matrix products: 10.6 us -> 18.5 us  [the longest x4 5.29 us: expert_half(): gate_part += jnp.dot(block, gate_rows, preferred_element_type=jnp.float32)]
    scatter x2 -> x0, local copies, waits for them, and re-layouts: 4.89 us -> none  [the longest x1 2.45 us: expert_half(): source_row = jnp.zeros((expert_count * capacity,), jnp.int32).at[target]....]
    select_n x3 -> x0, other arithmetic: 4.48 us -> none  [the longest x1 4.47 us: expert_half(): jnp.where(occupied[:, None] > 0, normed[source_row], jnp.zeros((), jnp.bf...]
  transfers between devices with their start and end apart: 5 -> 10, of which waited for: 2 -> 6; matrix products, arithmetic and copies ran while one was open for 18% -> 25% of each run, Pallas kernels for 0% -> 0%
where the time goes in v1:
time: 180 us; the launch traced here: 179 us
  waiting for transfers between devices  88 us (49%)
  matrix products  40 us (22%)
  starting transfers between devices  15 us (8%)
  between operations  14.5 us (8%)
  other arithmetic  11.3 us (6%)
  local copies, waits for them, and re-layouts  10.7 us (6%)
    all_to_all x1, waiting for transfers between devices, attention_half(): lax.all_to_all(outgoing, 'ep', split_axis=0, concat_axis=0, tiled=True)  27.4 us
    ppermute x6, waiting for transfers between devices, swap(): return lax.ppermute(block, 'tp', [(i, i ^ distance) for i in range(count)])  27.3 us
    all_to_all x1, waiting for transfers between devices, expert_half(): lax.all_to_all(summed.reshape(expert_count, capacity, part_width), 'ep',...  19.9 us
    all_gather x1, waiting for transfers between devices, attention_half(): joined = lax.all_gather(compact, 'ep', axis=0, tiled=True)  12.1 us
    all_to_all x1, starting transfers between devices, attention_half(): lax.all_to_all(outgoing, 'ep', split_axis=0, concat_axis=0, tiled=True)  7.32 us
    dot_general x4, matrix products, expert_half(): gate_part += jnp.dot(block, gate_rows, preferred_element_type=jnp.float32)  5.29 us
    dot_general x4, matrix products, expert_half(): jnp.dot(hidden, down_columns, preferred_element_type=jnp.float32)  4.72 us
    dot_general x4, matrix products, expert_half(): up_part += jnp.dot(block, up_rows, preferred_element_type=jnp.float32)  4.21 us
  transfers between devices with their start and end apart: 10, of which 6 were waited for; matrix products, arithmetic and copies ran while one was open for 25% of the time, Pallas kernels for 0%

profile of v1, /device:TPU:0, one launch (start us, length us, event | category | flops | bytes accessed | tf_op | source)
XLA Modules:
  0.0 179.4 jit_solution(13265398370250602035)
XLA Ops:
  13.3 2.2 %multiply_reduce_fusion.1 = (f32[128]{0:T(128)S(1)}, f32[128,512]{1,0:T(8,128)S(1)}) fusion(bf16[2048,512]{1,0:T(8,128)(2,1)} %param.21, bf16[128,2048]{1,0:T(8,128)(2,1)S(1)} %copy-done.6, f32[2048]{0:T(1024)S(1)} %copy-done.11, f32[128]{0:T(128)S(1)} %add_rsqrt_fusion.2), kind=kOutput, calls=%fused_computation.81 | convolution fusion | flops 269614976 | bytes 2892800 | tf_op jit(solution)/shard_map/dot_general | solution.py:64
  17.5 2.5 %convolution_convert_fusion.1 = bf16[1024,512]{1,0:T(8,128)(2,1)} fusion(pred[1024,256]{1,0:T(32,128)(4,1)S(1)} %bitcast_compare_fusion, f32[512]{0:T(512)S(1)} %dynamic_slice.67, f32[256]{0:T(256)S(1)} %add_rsqrt_fusion, bf16[256,2048]{1,0:T(8,128)(2,1)} %param.27, s32[]{:T(128)S(6)} %select_n.45), kind=kOutput, calls=%fused_computation.19 | convolution fusion | flops 269484032 | bytes 1575940 | tf_op jit(solution)/shard_map/dot_general | solution.py:147
  20.0 7.3 %all-to-all-start = ((bf16[8,128,512]{2,1,0:T(8,128)(2,1)}), bf16[8,128,512]{2,1,0:T(8,128)(2,1)S(1)}, u32[]{:S(2)}, u32[]{:S(2)}) async-start(bf16[8,128,512]{2,1,0:T(8,128)(2,1)} %bitcast.118), calls=%async_computation | async-start | bytes 2097152 | tf_op jit(solution)/shard_map/all_to_all | solution.py:73
  27.3 2.3 %convolution_convert_fusion.6 = bf16[128,512]{1,0:T(8,128)(2,1)S(1)} fusion(bf16[2048,512]{1,0:T(8,128)(2,1)} %param.19, bf16[128,2048]{1,0:T(8,128)(2,1)} %param.17, f32[2048]{0:T(1024)S(1)} %copy-done.11, f32[128]{0:T(128)S(1)} %add_rsqrt_fusion.2), kind=kOutput, calls=%fused_computation.36 | convolution fusion | flops 269549568 | bytes 2761216 | tf_op jit(solution)/shard_map/dot_general | solution.py:57
  29.8 2.0 %fusion.88 = f32[128,256]{0,1:T(8,128)S(1)} fusion(bf16[2048,256]{1,0:T(8,128)(2,1)} %param.20, bf16[128,2048]{1,0:T(8,128)(2,1)} %param.17, f32[2048]{0:T(1024)S(1)} %copy-done.11, f32[128]{0:T(128)S(1)} %add_rsqrt_fusion.2), kind=kOutput, calls=%fused_computation.142 | convolution fusion | flops 135266304 | bytes 1712640 | tf_op jit(solution)/shard_map/dot_general | solution.py:59
  31.9 27.4 %all-to-all-done = bf16[8,128,512]{2,1,0:T(8,128)(2,1)S(1)} async-done(((bf16[8,128,512]{2,1,0:T(8,128)(2,1)}), bf16[8,128,512]{2,1,0:T(8,128)(2,1)S(1)}, u32[]{:S(2)}, u32[]{:S(2)}) %all-to-all-start) | async-done | bytes 1048608 | tf_op jit(solution)/shard_map/all_to_all | solution.py:73
  59.3 12.1 %all-gather.2.cloned.1.call-done = bf16[1024,544]{1,0:T(8,128)(2,1)} async-done(((bf16[128,544]{1,0:T(8,128)(2,1)}), bf16[1024,544]{1,0:T(8,128)(2,1)}) %all-gather.2.cloned.1.call-update) | async-done | bytes 1114128 | tf_op jit(solution)/shard_map/all_gather | solution.py:72
  73.1 3.1 %convolution_convert_fusion.5 = bf16[1024,512]{1,0:T(8,128)(2,1)} fusion(bf16[512,512]{1,0:T(8,128)(2,1)} %param.24, bf16[1024,544]{1,0:T(8,128)(2,1)} %all-gather.2.cloned.1.call-done), kind=kOutput, calls=%fused_computation.23 | convolution fusion | flops 537395200 | bytes 2621440 | tf_op jit(solution)/shard_map/dot_general | solution.py:76
  76.2 3.9 %reshape.230 = bf16[8,128,8,64]{3,2,1,0:T(8,128)(2,1)} reshape(bf16[1024,512]{1,0:T(8,128)(2,1)} %convolution_convert_fusion.5) | data formatting | bytes 2097152 | tf_op jit(solution)/shard_map/reshape | solution.py:84
  80.1 1.5 fusion.44
  82.1 13.3 %collective-permute-done = bf16[1024,512]{1,0:T(8,128)(2,1)} collective-permute-done((bf16[1024,512]{1,0:T(8,128)(2,1)S(1)}, bf16[1024,512]{1,0:T(8,128)(2,1)}, u32[]{:S(2)}, u32[]{:S(2)}) %collective-permute-start) | collective-permute-done | bytes 1048608 | tf_op jit(solution)/shard_map/ppermute | solution.py:157
  95.4 1.7 convolution_add_fusion.5
  97.0 1.7 convolution_add_fusion.2
  98.7 1.7 convolution_add_fusion.4
  100.4 1.7 convolution_add_fusion.1
  105.7 2.9 %fusion.96 = (f32[128,8,8]{0,2,1:T(8,128)S(1)}, f32[128,8,8,128]{0,3,2,1:T(8,128)}) fusion(bf16[8,128,32,1]{2,1,0,3:T(8,128)(2,1)S(1)} %bitcast.119, bf16[128,8,16]{0,2,1:T(8,128)(2,1)S(1)} %get-tuple-element.17, bf16[128,8,16]{0,2,1:T(8,128)(2,1)S(1)} %get-tuple-element.16, f32[8,8,128,128]{3,2,1,0:T(8,128)S(1)} %fusion.8, ...), kind=kOutput, calls=%fused_computation.146 | convolution fusion | flops 71426048 | bytes 8683520 | tf_op jit(solution)/shard_map/yjx,inx->yjin/dot_general | solution.py:89
  113.2 1.7 convolution_convert_fusion.4
  114.9 3.9 %reshape.231 = bf16[8,128,8,64]{3,2,1,0:T(8,128)(2,1)} reshape(bf16[1024,512]{1,0:T(8,128)(2,1)} %convolution_convert_fusion.4) | data formatting | bytes 2097152 | tf_op jit(solution)/shard_map/reshape | solution.py:85
  118.8 3.2 %fusion.2 = (f32[128,8,8]{0,2,1:T(8,128)S(1)}, f32[128,8]{0,1:T(8,128)S(1)}) fusion(f32[128,8,8,128]{0,3,2,1:T(8,128)} %get-tuple-element.32, f32[128,8,8]{0,2,1:T(8,128)S(1)} %get-tuple-element.31, pred[128,8,128]{0,2,1:T(8,128)(4,1)S(1)} %broadcast_compare_fusion), kind=kLoop, calls=%fused_computation.4 | loop fusion | flops 4185088 | bytes 4395008 | tf_op jit(solution)/shard_map/reduce_sum | solution.py:101
  123.4 14.0 %collective-permute-done.5 = bf16[1024,512]{1,0:T(8,128)(2,1)} collective-permute-done((bf16[1024,512]{1,0:T(8,128)(2,1)}, bf16[1024,512]{1,0:T(8,128)(2,1)}, u32[]{:S(2)}, u32[]{:S(2)}) %collective-permute-start.5) | collective-permute-done | bytes 1048608 | tf_op jit(solution)/shard_map/ppermute | solution.py:157
  137.4 3.0 %add_convert_fusion = bf16[1024,512]{1,0:T(8,128)(2,1)} fusion(bf16[1024,512]{1,0:T(8,128)(2,1)} %collective-permute-done.5, f32[1024,512]{1,0:T(8,128)S(1)} %fusion.32, bf16[1024,512]{1,0:T(8,128)(2,1)} %collective-permute-done.3), kind=kLoop, calls=%fused_computation.13 | loop fusion | flops 2621440 | bytes 5242880 | tf_op jit(solution)/shard_map/convert_element_type | solution.py:191
  140.5 3.6 %all-to-all-start.1 = ((bf16[8,128,512]{2,1,0:T(8,128)(2,1)}), bf16[8,128,512]{2,1,0:T(8,128)(2,1)S(1)}, u32[]{:S(2)}, u32[]{:S(2)}) async-start(bf16[8,128,512]{2,1,0:T(8,128)(2,1)} %bitcast.33), calls=%async_computation.2 | async-start | bytes 2097152 | tf_op jit(solution)/shard_map/all_to_all | solution.py:192
  144.3 4.0 %fusion.6 = f32[128,8,64]{0,2,1:T(8,128)S(1)} fusion(f32[128,8,8]{0,2,1:T(8,128)S(1)} %get-tuple-element.15, f32[128,8,8,128]{0,3,2,1:T(8,128)} %get-tuple-element.32, f32[128,8,8]{0,2,1:T(8,128)S(1)} %get-tuple-element.31, pred[128,8,128]{0,2,1:T(8,128)(4,1)S(1)} %broadcast_compare_fusion, bf16[8,128,8,64]{3,2,1,0:T(8,128)(2,1)} %reshape.231), kind=kOutput, calls=%fused_computation.9 | convolution fusion | flops 138346496 | bytes 5701632 | tf_op jit(solution)/shard_map/qhbk,bkhd->qhbd/dot_general | solution.py:102
  149.7 19.9 %all-to-all-done.1 = bf16[8,128,512]{2,1,0:T(8,128)(2,1)S(1)} async-done(((bf16[8,128,512]{2,1,0:T(8,128)(2,1)}), bf16[8,128,512]{2,1,0:T(8,128)(2,1)S(1)}, u32[]{:S(2)}, u32[]{:S(2)}) %all-to-all-start.1) | async-done | bytes 1048608 | tf_op jit(solution)/shard_map/all_to_all | solution.py:192
  (83 shorter events, 24.6 us)
Async XLA Ops:
  7.2 141.2 %copy-start = (bf16[512,2048]{1,0:T(8,128)(2,1)S(1)}, bf16[512,2048]{1,0:T(8,128)(2,1)}, u32[]{:S(2)}) copy-start(bf16[512,2048]{1,0:T(8,128)(2,1)} %param.26) | copy-start | bytes 6291460
  7.2 6.1 %copy-start.6 = (bf16[128,2048]{1,0:T(8,128)(2,1)S(1)}, bf16[128,2048]{1,0:T(8,128)(2,1)}, u32[]{:S(2)}) copy-start(bf16[128,2048]{1,0:T(8,128)(2,1)} %param.17) | copy-start | bytes 1572868
  7.2 6.1 %copy-start.11 = (f32[2048]{0:T(1024)S(1)}, f32[2048]{0:T(1024)}, u32[]{:S(2)}) copy-start(f32[2048]{0:T(1024)} %param.18) | copy-start | bytes 24580
  7.2 64.2 %all-gather.2.cloned.1.call-start = ((), (), s32[]{:S(2)}) async-start(), calls=%async_computation.3 | async-start | bytes 1474560 | tf_op jit(solution)/shard_map/all_gather | solution.py:72
  11.6 5.1 %copy-start.9 = (f32[512]{0:T(512)S(1)}, f32[512]{0:T(512)}, u32[]{:S(2)}) copy-start(f32[512]{0:T(512)} %param.23) | copy-start | bytes 6148
  20.0 9.7 %copy-start.8 = (f32[256,2]{0,1:T(2,128)S(1)}, f32[256,2]{0,1:T(2,128)}, u32[]{:S(2)}) copy-start(f32[256,2]{0,1:T(2,128)} %param.30) | copy-start | bytes 6148
  20.0 39.3 %all-to-all-start = ((bf16[8,128,512]{2,1,0:T(8,128)(2,1)}), bf16[8,128,512]{2,1,0:T(8,128)(2,1)S(1)}, u32[]{:S(2)}, u32[]{:S(2)}) async-start(bf16[8,128,512]{2,1,0:T(8,128)(2,1)} %bitcast.118), calls=%async_computation | async-start | bytes 2097152 | tf_op jit(solution)/shard_map/all_to_all | solution.py:73
  71.4 24.0 %collective-permute-start = (bf16[1024,512]{1,0:T(8,128)(2,1)S(1)}, bf16[1024,512]{1,0:T(8,128)(2,1)}, u32[]{:S(2)}, u32[]{:S(2)}) collective-permute-start(bf16[1024,512]{1,0:T(8,128)(2,1)S(1)} %bitcast.114), channel_id=1, source_target_pairs={{0,2},{1,3},{2,0},{3,1},{4,6},{5,7},{6,4},{7,5},{8,10},{9,11},{10,... | collective-permute-start | bytes 3145736 | tf_op jit(solution)/shard_map/ppermute | solution.py:157
  73.1 25.7 %collective-permute-start.1 = (bf16[1024,512]{1,0:T(8,128)(2,1)S(1)}, bf16[1024,512]{1,0:T(8,128)(2,1)}, u32[]{:S(2)}, u32[]{:S(2)}) collective-permute-start(bf16[1024,512]{1,0:T(8,128)(2,1)S(1)} %bitcast.115), channel_id=1, source_target_pairs={{0,1},{1,0},{2,3},{3,2},{4,5},{5,4},{6,7},{7,6},{8,9},{9,8},{10,11... | collective-permute-start | bytes 3145736 | tf_op jit(solution)/shard_map/ppermute | solution.py:157
  80.1 1.5 copy-start.5
  80.1 15.3 %copy-start.2 = (bf16[1,2048,256]{2,1,0:T(8,128)(2,1)S(1)}, bf16[1,2048,256]{2,1,0:T(8,128)(2,1)}, u32[]{:S(2)}) copy-start(bf16[1,2048,256]{2,1,0:T(8,128)(2,1)} %param.31) | copy-start | bytes 3145732
  95.4 6.7 %collective-permute-start.2 = (bf16[1024,512]{1,0:T(8,128)(2,1)}, bf16[1024,512]{1,0:T(8,128)(2,1)S(1)}, u32[]{:S(2)}, u32[]{:S(2)}) collective-permute-start(bf16[1024,512]{1,0:T(8,128)(2,1)} %collective-permute-done), channel_id=1, source_target_pairs={{0,1},{1,0},{2,3},{3,2},{4,5},{5,4},{6,7},{7,6},{8,9},{9,8},{10,11... | collective-permute-start | bytes 3145736 | tf_op jit(solution)/shard_map/ppermute | solution.py:157
  102.5 1.2 copy-start.4
  102.5 2.2 %copy-start.1 = (bf16[8,128,8,64]{3,2,1,0:T(8,128)(2,1)S(1)}, bf16[8,128,8,64]{3,2,1,0:T(8,128)(2,1)}, u32[]{:S(2)}) copy-start(bf16[8,128,8,64]{3,2,1,0:T(8,128)(2,1)} %reshape.230) | copy-start | bytes 3145732
  104.2 6.1 %collective-permute-start.4 = (bf16[1024,512]{1,0:T(8,128)(2,1)S(1)}, bf16[1024,512]{1,0:T(8,128)(2,1)S(1)}, u32[]{:S(2)}, u32[]{:S(2)}) collective-permute-start(bf16[1024,512]{1,0:T(8,128)(2,1)S(1)} %convolution_convert_fusion.2), channel_id=1, source_target_pairs={{0,1},{1,0},{2,3},{3,2},{4,5},{5,4},{6,7},{7,6},{8,9},{9,8},{10,11... | collective-permute-start | bytes 3145736 | tf_op jit(solution)/shard_map/ppermute | solution.py:157
  104.8 1.0 slice-start
  108.6 4.6 %copy-start.3 = (bf16[1024,544]{1,0:T(8,128)(2,1)S(1)}, bf16[1024,544]{1,0:T(8,128)(2,1)}, u32[]{:S(2)}) copy-start(bf16[1024,544]{1,0:T(8,128)(2,1)} %all-gather.2.cloned.1.call-done) | copy-start | bytes 3342340
  108.6 4.6 %copy-start.10 = (bf16[512,512]{1,0:T(8,128)(2,1)S(1)}, bf16[512,512]{1,0:T(8,128)(2,1)}, u32[]{:S(2)}) copy-start(bf16[512,512]{1,0:T(8,128)(2,1)} %param.25) | copy-start | bytes 1572868
  110.1 13.3 %collective-permute-start.3 = (bf16[1024,512]{1,0:T(8,128)(2,1)}, bf16[1024,512]{1,0:T(8,128)(2,1)}, u32[]{:S(2)}, u32[]{:S(2)}) collective-permute-start(bf16[1024,512]{1,0:T(8,128)(2,1)} %convolution_convert_fusion.3), channel_id=1, source_target_pairs={{0,1},{1,0},{2,3},{3,2},{4,5},{5,4},{6,7},{7,6},{8,9},{9,8},{10,11... | collective-permute-start | bytes 3145736 | tf_op jit(solution)/shard_map/ppermute | solution.py:157
  111.7 25.7 %collective-permute-start.5 = (bf16[1024,512]{1,0:T(8,128)(2,1)}, bf16[1024,512]{1,0:T(8,128)(2,1)}, u32[]{:S(2)}, u32[]{:S(2)}) collective-permute-start(bf16[1024,512]{1,0:T(8,128)(2,1)} %add_convert_fusion.1), channel_id=1, source_target_pairs={{0,2},{1,3},{2,0},{3,1},{4,6},{5,7},{6,4},{7,5},{8,10},{9,11},{10,... | collective-permute-start | bytes 3145736 | tf_op jit(solution)/shard_map/ppermute | solution.py:157
  140.5 29.2 %all-to-all-start.1 = ((bf16[8,128,512]{2,1,0:T(8,128)(2,1)}), bf16[8,128,512]{2,1,0:T(8,128)(2,1)S(1)}, u32[]{:S(2)}, u32[]{:S(2)}) async-start(bf16[8,128,512]{2,1,0:T(8,128)(2,1)} %bitcast.33), calls=%async_computation.2 | async-start | bytes 2097152 | tf_op jit(solution)/shard_map/all_to_all | solution.py:192
  144.0 28.5 %reduce-scatter.2.cloned.1.call-start = ((), (), s32[]{:S(2)}) async-start(), calls=%async_computation.4 | async-start | bytes 655360 | tf_op jit(solution)/shard_map/reduce_scatter | solution.py:116
  148.3 1.4 copy-start.7
Sparse Core Ops, SparseCore 0:
  20.1 51.2 all-gather.1
  149.8 22.7 reduce-scatter.1

commit v2 on v1

--- a/solution.py
+++ b/solution.py
@@ -71,7 +71,6 @@
     )
     joined = lax.all_gather(compact, "ep", axis=0, tiled=True)
     arrived = lax.all_to_all(outgoing, "ep", split_axis=0, concat_axis=0, tiled=True)
-    joined, arrived = lax.optimization_barrier((joined, arrived))
     pieces = (joined[:, : latent.shape[1]], joined[:, latent.shape[1] :])
     piece_keys = jnp.dot(pieces[0], w_key_up, preferred_element_type=jnp.float32).astype(
         jnp.bfloat16

time: 180 us -> 172 us (0.956)
  waiting for transfers between devices: 88 us -> 76 us
  matrix products: 40 us -> 43.4 us
    ppermute x6, waiting for transfers between devices: 27.3 us -> 14 us  [swap(): return lax.ppermute(block, 'tp', [(i, i ^ distance) for i in range(count)])]
    all_gather x1, waiting for transfers between devices: 12.1 us -> 14.4 us  [attention_half(): joined = lax.all_gather(compact, 'ep', axis=0, tiled=True)]
    dot_general x4, matrix products: 4.21 us -> 6.22 us  [expert_half(): up_part += jnp.dot(block, up_rows, preferred_element_type=jnp.float32)]
  transfers between devices with their start and end apart: 10 -> 10, of which waited for: 6 -> 5; matrix products, arithmetic and copies ran while one was open for 25% -> 28% of each run, Pallas kernels for 0% -> 0%
where the time goes in v2:
time: 172 us; the launch traced here: 171 us
  waiting for transfers between devices  76 us (44%)
  matrix products  43.4 us (25%)
  starting transfers between devices  14.9 us (9%)
  between operations  14.5 us (8%)
  other arithmetic  11.3 us (7%)
  local copies, waits for them, and re-layouts  10.7 us (6%)
    all_to_all x1, waiting for transfers between devices, attention_half(): lax.all_to_all(outgoing, 'ep', split_axis=0, concat_axis=0, tiled=True)  25.7 us
    all_to_all x1, waiting for transfers between devices, expert_half(): lax.all_to_all(summed.reshape(expert_count, capacity, part_width), 'ep',...  19.9 us
    all_gather x1, waiting for transfers between devices, attention_half(): joined = lax.all_gather(compact, 'ep', axis=0, tiled=True)  14.4 us
    ppermute x6, waiting for transfers between devices, swap(): return lax.ppermute(block, 'tp', [(i, i ^ distance) for i in range(count)])  14 us
    all_to_all x1, starting transfers between devices, attention_half(): lax.all_to_all(outgoing, 'ep', split_axis=0, concat_axis=0, tiled=True)  7.31 us
    dot_general x4, matrix products, expert_half(): gate_part += jnp.dot(block, gate_rows, preferred_element_type=jnp.float32)  6.69 us
    dot_general x4, matrix products, expert_half(): up_part += jnp.dot(block, up_rows, preferred_element_type=jnp.float32)  6.22 us
    dot_general x4, matrix products, expert_half(): jnp.dot(hidden, down_columns, preferred_element_type=jnp.float32)  4.71 us
  transfers between devices with their start and end apart: 10, of which 5 were waited for; matrix products, arithmetic and copies ran while one was open for 28% of the time, Pallas kernels for 0%

profile of v2, /device:TPU:0, one launch (start us, length us, event | category | flops | bytes accessed | tf_op | source)
XLA Modules:
  0.0 170.8 jit_solution(8710696470042588831)
XLA Ops:
  13.3 2.2 %multiply_reduce_fusion.1 = (f32[128]{0:T(128)S(1)}, f32[128,512]{1,0:T(8,128)S(1)}) fusion(bf16[2048,512]{1,0:T(8,128)(2,1)} %param.21, bf16[128,2048]{1,0:T(8,128)(2,1)S(1)} %copy-done.7, f32[2048]{0:T(1024)S(1)} %copy-done.12, f32[128]{0:T(128)S(1)} %add_rsqrt_fusion.2), kind=kOutput, calls=%fused_computation.81 | convolution fusion | flops 269614976 | bytes 2892800 | tf_op jit(solution)/shard_map/dot_general | solution.py:64
  17.4 2.5 %convolution_convert_fusion.1 = bf16[1024,512]{1,0:T(8,128)(2,1)} fusion(pred[1024,256]{1,0:T(32,128)(4,1)S(1)} %bitcast_compare_fusion, f32[512]{0:T(512)S(1)} %dynamic_slice.67, f32[256]{0:T(256)S(1)} %add_rsqrt_fusion, bf16[256,2048]{1,0:T(8,128)(2,1)} %param.27, s32[]{:T(128)S(6)} %select_n.45), kind=kOutput, calls=%fused_computation.19 | convolution fusion | flops 269484032 | bytes 1575940 | tf_op jit(solution)/shard_map/dot_general | solution.py:146
  19.9 7.3 %all-to-all-start = ((bf16[8,128,512]{2,1,0:T(8,128)(2,1)}), bf16[8,128,512]{2,1,0:T(8,128)(2,1)S(1)}, u32[]{:S(2)}, u32[]{:S(2)}) async-start(bf16[8,128,512]{2,1,0:T(8,128)(2,1)} %bitcast.118), calls=%async_computation.1 | async-start | bytes 2097152 | tf_op jit(solution)/shard_map/all_to_all | solution.py:73
  28.0 2.3 %convolution_convert_fusion.6 = bf16[128,512]{1,0:T(8,128)(2,1)S(1)} fusion(bf16[2048,512]{1,0:T(8,128)(2,1)} %param.19, bf16[128,2048]{1,0:T(8,128)(2,1)} %param.17, f32[2048]{0:T(1024)S(1)} %copy-done.12, f32[128]{0:T(128)S(1)} %add_rsqrt_fusion.2), kind=kOutput, calls=%fused_computation.36 | convolution fusion | flops 269549568 | bytes 2761216 | tf_op jit(solution)/shard_map/dot_general | solution.py:57
  30.5 2.0 %fusion.88 = f32[128,256]{0,1:T(8,128)S(1)} fusion(bf16[2048,256]{1,0:T(8,128)(2,1)} %param.20, bf16[128,2048]{1,0:T(8,128)(2,1)} %param.17, f32[2048]{0:T(1024)S(1)} %copy-done.12, f32[128]{0:T(128)S(1)} %add_rsqrt_fusion.2), kind=kOutput, calls=%fused_computation.142 | convolution fusion | flops 135266304 | bytes 1712640 | tf_op jit(solution)/shard_map/dot_general | solution.py:59
  32.5 25.7 %all-to-all-done = bf16[8,128,512]{2,1,0:T(8,128)(2,1)S(1)} async-done(((bf16[8,128,512]{2,1,0:T(8,128)(2,1)}), bf16[8,128,512]{2,1,0:T(8,128)(2,1)S(1)}, u32[]{:S(2)}, u32[]{:S(2)}) %all-to-all-start) | async-done | bytes 1048608 | tf_op jit(solution)/shard_map/all_to_all | solution.py:73
  60.0 2.4 %fusion.44 = f32[1024,256]{1,0:T(8,128)} fusion(bf16[1024,512]{1,0:T(8,128)(2,1)S(1)} %bitcast.116, bf16[1,2048,256]{2,1,0:T(8,128)(2,1)} %param.31, s32[]{:T(128)S(6)} %select_n.45), kind=kOutput, calls=%fused_computation.65 | convolution fusion | flops 268435456 | bytes 2359300 | tf_op jit(solution)/shard_map/dot_general | solution.py:177
  62.4 2.4 %fusion.39 = f32[1024,256]{1,0:T(8,128)} fusion(bf16[1024,512]{1,0:T(8,128)(2,1)S(1)} %bitcast.117, bf16[1,2048,256]{2,1,0:T(8,128)(2,1)} %param.32, s32[]{:T(128)S(6)} %select_n.45), kind=kOutput, calls=%fused_computation.60 | convolution fusion | flops 268435456 | bytes 2359300 | tf_op jit(solution)/shard_map/dot_general | solution.py:178
  64.8 14.4 %all-gather.2.cloned.1.call-done = bf16[1024,544]{1,0:T(8,128)(2,1)} async-done(((bf16[128,544]{1,0:T(8,128)(2,1)}), bf16[1024,544]{1,0:T(8,128)(2,1)}) %all-gather.2.cloned.1.call-update) | async-done | bytes 1114128 | tf_op jit(solution)/shard_map/all_gather | solution.py:72
  79.2 3.1 %convolution_convert_fusion.5 = bf16[1024,512]{1,0:T(8,128)(2,1)} fusion(bf16[512,512]{1,0:T(8,128)(2,1)} %param.24, bf16[1024,544]{1,0:T(8,128)(2,1)} %all-gather.2.cloned.1.call-done), kind=kOutput, calls=%fused_computation.23 | convolution fusion | flops 537395200 | bytes 2621440 | tf_op jit(solution)/shard_map/dot_general | solution.py:75
  82.3 3.9 %reshape.230 = bf16[8,128,8,64]{3,2,1,0:T(8,128)(2,1)} reshape(bf16[1024,512]{1,0:T(8,128)(2,1)} %convolution_convert_fusion.5) | data formatting | bytes 2097152 | tf_op jit(solution)/shard_map/reshape | solution.py:83
  86.3 2.2 %convolution_add_fusion.5 = f32[1024,256]{1,0:T(8,128)S(1)} fusion(f32[1024,256]{1,0:T(8,128)} %fusion.44, bf16[1024,512]{1,0:T(8,128)(2,1)} %collective-permute-done, bf16[1,2048,256]{2,1,0:T(8,128)(2,1)} %param.31, s32[]{:T(128)S(6)} %select_n.49), kind=kOutput, calls=%fused_computation.29 | convolution fusion | flops 268697600 | bytes 3407876 | tf_op jit(solution)/shard_map/dot_general | solution.py:177
  88.5 1.7 %convolution_add_fusion.2 = f32[1024,256]{1,0:T(8,128)S(1)} fusion(f32[1024,256]{1,0:T(8,128)S(1)} %copy-done.2, bf16[1024,512]{1,0:T(8,128)(2,1)} %collective-permute-done, bf16[1,2048,256]{2,1,0:T(8,128)(2,1)S(1)} %copy-done.6, s32[]{:T(128)S(6)} %select_n.49), kind=kOutput, calls=%fused_computation.26 | convolution fusion | flops 268697600 | bytes 3407876 | tf_op jit(solution)/shard_map/dot_general | solution.py:178
  90.2 1.7 convolution_add_fusion.4
  91.9 1.7 convolution_add_fusion.1
  97.1 2.9 %fusion.96 = (f32[128,8,8]{0,2,1:T(8,128)S(1)}, f32[128,8,8,128]{0,3,2,1:T(8,128)}) fusion(bf16[8,128,32,1]{2,1,0,3:T(8,128)(2,1)S(1)} %bitcast.119, bf16[128,8,16]{0,2,1:T(8,128)(2,1)S(1)} %get-tuple-element.13, bf16[128,8,16]{0,2,1:T(8,128)(2,1)S(1)} %get-tuple-element.12, f32[8,8,128,128]{3,2,1,0:T(8,128)S(1)} %fusion.8, ...), kind=kOutput, calls=%fused_computation.146 | convolution fusion | flops 71426048 | bytes 8683520 | tf_op jit(solution)/shard_map/yjx,inx->yjin/dot_general | solution.py:88
  104.6 1.7 convolution_convert_fusion.4
  106.3 3.9 %reshape.231 = bf16[8,128,8,64]{3,2,1,0:T(8,128)(2,1)} reshape(bf16[1024,512]{1,0:T(8,128)(2,1)} %convolution_convert_fusion.4) | data formatting | bytes 2097152 | tf_op jit(solution)/shard_map/reshape | solution.py:84
  110.2 3.2 %fusion.2 = (f32[128,8,8]{0,2,1:T(8,128)S(1)}, f32[128,8]{0,1:T(8,128)S(1)}) fusion(f32[128,8,8,128]{0,3,2,1:T(8,128)} %get-tuple-element.28, f32[128,8,8]{0,2,1:T(8,128)S(1)} %get-tuple-element.27, pred[128,8,128]{0,2,1:T(8,128)(4,1)S(1)} %broadcast_compare_fusion), kind=kLoop, calls=%fused_computation.4 | loop fusion | flops 4185088 | bytes 4395008 | tf_op jit(solution)/shard_map/reduce_sum | solution.py:100
  114.8 14.0 %collective-permute-done.5 = bf16[1024,512]{1,0:T(8,128)(2,1)} collective-permute-done((bf16[1024,512]{1,0:T(8,128)(2,1)}, bf16[1024,512]{1,0:T(8,128)(2,1)}, u32[]{:S(2)}, u32[]{:S(2)}) %collective-permute-start.5) | collective-permute-done | bytes 1048608 | tf_op jit(solution)/shard_map/ppermute | solution.py:156
  128.8 3.0 %add_convert_fusion = bf16[1024,512]{1,0:T(8,128)(2,1)} fusion(bf16[1024,512]{1,0:T(8,128)(2,1)} %collective-permute-done.5, f32[1024,512]{1,0:T(8,128)S(1)} %fusion.32, bf16[1024,512]{1,0:T(8,128)(2,1)} %collective-permute-done.3), kind=kLoop, calls=%fused_computation.13 | loop fusion | flops 2621440 | bytes 5242880 | tf_op jit(solution)/shard_map/convert_element_type | solution.py:190
  131.9 3.7 %all-to-all-start.1 = ((bf16[8,128,512]{2,1,0:T(8,128)(2,1)}), bf16[8,128,512]{2,1,0:T(8,128)(2,1)S(1)}, u32[]{:S(2)}, u32[]{:S(2)}) async-start(bf16[8,128,512]{2,1,0:T(8,128)(2,1)} %bitcast.33), calls=%async_computation.2 | async-start | bytes 2097152 | tf_op jit(solution)/shard_map/all_to_all | solution.py:191
  135.7 4.0 %fusion.6 = f32[128,8,64]{0,2,1:T(8,128)S(1)} fusion(f32[128,8,8]{0,2,1:T(8,128)S(1)} %get-tuple-element.11, f32[128,8,8,128]{0,3,2,1:T(8,128)} %get-tuple-element.28, f32[128,8,8]{0,2,1:T(8,128)S(1)} %get-tuple-element.27, pred[128,8,128]{0,2,1:T(8,128)(4,1)S(1)} %broadcast_compare_fusion, bf16[8,128,8,64]{3,2,1,0:T(8,128)(2,1)} %reshape.231), kind=kOutput, calls=%fused_computation.9 | convolution fusion | flops 138346496 | bytes 5701632 | tf_op jit(solution)/shard_map/qhbk,bkhd->qhbd/dot_general | solution.py:101
  141.1 19.9 %all-to-all-done.1 = bf16[8,128,512]{2,1,0:T(8,128)(2,1)S(1)} async-done(((bf16[8,128,512]{2,1,0:T(8,128)(2,1)}), bf16[8,128,512]{2,1,0:T(8,128)(2,1)S(1)}, u32[]{:S(2)}, u32[]{:S(2)}) %all-to-all-start.1) | async-done | bytes 1048608 | tf_op jit(solution)/shard_map/all_to_all | solution.py:191
  (86 shorter events, 24.6 us)
Async XLA Ops:
  7.2 132.5 %copy-start = (bf16[512,2048]{1,0:T(8,128)(2,1)S(1)}, bf16[512,2048]{1,0:T(8,128)(2,1)}, u32[]{:S(2)}) copy-start(bf16[512,2048]{1,0:T(8,128)(2,1)} %param.26) | copy-start | bytes 6291460
  7.2 6.1 %copy-start.7 = (bf16[128,2048]{1,0:T(8,128)(2,1)S(1)}, bf16[128,2048]{1,0:T(8,128)(2,1)}, u32[]{:S(2)}) copy-start(bf16[128,2048]{1,0:T(8,128)(2,1)} %param.17) | copy-start | bytes 1572868
  7.2 6.1 %copy-start.12 = (f32[2048]{0:T(1024)S(1)}, f32[2048]{0:T(1024)}, u32[]{:S(2)}) copy-start(f32[2048]{0:T(1024)} %param.18) | copy-start | bytes 24580
  11.5 5.1 %copy-start.10 = (f32[512]{0:T(512)S(1)}, f32[512]{0:T(512)}, u32[]{:S(2)}) copy-start(f32[512]{0:T(512)} %param.23) | copy-start | bytes 6148
  19.9 38.3 %all-to-all-start = ((bf16[8,128,512]{2,1,0:T(8,128)(2,1)}), bf16[8,128,512]{2,1,0:T(8,128)(2,1)S(1)}, u32[]{:S(2)}, u32[]{:S(2)}) async-start(bf16[8,128,512]{2,1,0:T(8,128)(2,1)} %bitcast.118), calls=%async_computation.1 | async-start | bytes 2097152 | tf_op jit(solution)/shard_map/all_to_all | solution.py:73
  27.2 3.2 %copy-start.9 = (f32[256,2]{0,1:T(2,128)S(1)}, f32[256,2]{0,1:T(2,128)}, u32[]{:S(2)}) copy-start(f32[256,2]{0,1:T(2,128)} %param.30) | copy-start | bytes 6148
  27.2 52.0 %all-gather.2.cloned.1.call-start = ((), (), s32[]{:S(2)}) async-start(), calls=%async_computation.3 | async-start | bytes 1474560 | tf_op jit(solution)/shard_map/all_gather | solution.py:72
  58.2 27.9 %collective-permute-start = (bf16[1024,512]{1,0:T(8,128)(2,1)S(1)}, bf16[1024,512]{1,0:T(8,128)(2,1)}, u32[]{:S(2)}, u32[]{:S(2)}) collective-permute-start(bf16[1024,512]{1,0:T(8,128)(2,1)S(1)} %bitcast.114), channel_id=1, source_target_pairs={{0,2},{1,3},{2,0},{3,1},{4,6},{5,7},{6,4},{7,5},{8,10},{9,11},{10,... | collective-permute-start | bytes 3145736 | tf_op jit(solution)/shard_map/ppermute | solution.py:156
  59.9 30.3 %collective-permute-start.1 = (bf16[1024,512]{1,0:T(8,128)(2,1)S(1)}, bf16[1024,512]{1,0:T(8,128)(2,1)}, u32[]{:S(2)}, u32[]{:S(2)}) collective-permute-start(bf16[1024,512]{1,0:T(8,128)(2,1)S(1)} %bitcast.115), channel_id=1, source_target_pairs={{0,1},{1,0},{2,3},{3,2},{4,5},{5,4},{6,7},{7,6},{8,9},{9,8},{10,11... | collective-permute-start | bytes 3145736 | tf_op jit(solution)/shard_map/ppermute | solution.py:156
  86.2 2.3 %copy-start.2 = (f32[1024,256]{1,0:T(8,128)S(1)}, f32[1024,256]{1,0:T(8,128)}, u32[]{:S(2)}) copy-start(f32[1024,256]{1,0:T(8,128)} %fusion.39) | copy-start | bytes 3145732
  86.2 2.3 %copy-start.6 = (bf16[1,2048,256]{2,1,0:T(8,128)(2,1)S(1)}, bf16[1,2048,256]{2,1,0:T(8,128)(2,1)}, u32[]{:S(2)}) copy-start(bf16[1,2048,256]{2,1,0:T(8,128)(2,1)} %param.32) | copy-start | bytes 3145732
  86.2 7.4 %collective-permute-start.2 = (bf16[1024,512]{1,0:T(8,128)(2,1)}, bf16[1024,512]{1,0:T(8,128)(2,1)S(1)}, u32[]{:S(2)}, u32[]{:S(2)}) collective-permute-start(bf16[1024,512]{1,0:T(8,128)(2,1)} %collective-permute-done), channel_id=1, source_target_pairs={{0,1},{1,0},{2,3},{3,2},{4,5},{5,4},{6,7},{7,6},{8,9},{9,8},{10,11... | collective-permute-start | bytes 3145736 | tf_op jit(solution)/shard_map/ppermute | solution.py:156
  88.5 1.8 %copy-start.3 = (bf16[1,2048,256]{2,1,0:T(8,128)(2,1)S(1)}, bf16[1,2048,256]{2,1,0:T(8,128)(2,1)}, u32[]{:S(2)}) copy-start(bf16[1,2048,256]{2,1,0:T(8,128)(2,1)} %param.31) | copy-start | bytes 3145732
  94.1 1.2 copy-start.5
  94.1 2.1 %copy-start.1 = (bf16[8,128,8,64]{3,2,1,0:T(8,128)(2,1)S(1)}, bf16[8,128,8,64]{3,2,1,0:T(8,128)(2,1)}, u32[]{:S(2)}) copy-start(bf16[8,128,8,64]{3,2,1,0:T(8,128)(2,1)} %reshape.230) | copy-start | bytes 3145732
  95.7 6.0 %collective-permute-start.4 = (bf16[1024,512]{1,0:T(8,128)(2,1)S(1)}, bf16[1024,512]{1,0:T(8,128)(2,1)S(1)}, u32[]{:S(2)}, u32[]{:S(2)}) collective-permute-start(bf16[1024,512]{1,0:T(8,128)(2,1)S(1)} %convolution_convert_fusion.2), channel_id=1, source_target_pairs={{0,1},{1,0},{2,3},{3,2},{4,5},{5,4},{6,7},{7,6},{8,9},{9,8},{10,11... | collective-permute-start | bytes 3145736 | tf_op jit(solution)/shard_map/ppermute | solution.py:156
  96.2 1.0 slice-start
  100.0 4.6 %copy-start.4 = (bf16[1024,544]{1,0:T(8,128)(2,1)S(1)}, bf16[1024,544]{1,0:T(8,128)(2,1)}, u32[]{:S(2)}) copy-start(bf16[1024,544]{1,0:T(8,128)(2,1)} %all-gather.2.cloned.1.call-done) | copy-start | bytes 3342340
  100.0 4.6 %copy-start.11 = (bf16[512,512]{1,0:T(8,128)(2,1)S(1)}, bf16[512,512]{1,0:T(8,128)(2,1)}, u32[]{:S(2)}) copy-start(bf16[512,512]{1,0:T(8,128)(2,1)} %param.25) | copy-start | bytes 1572868
  101.5 13.3 %collective-permute-start.3 = (bf16[1024,512]{1,0:T(8,128)(2,1)}, bf16[1024,512]{1,0:T(8,128)(2,1)}, u32[]{:S(2)}, u32[]{:S(2)}) collective-permute-start(bf16[1024,512]{1,0:T(8,128)(2,1)} %convolution_convert_fusion.3), channel_id=1, source_target_pairs={{0,1},{1,0},{2,3},{3,2},{4,5},{5,4},{6,7},{7,6},{8,9},{9,8},{10,11... | collective-permute-start | bytes 3145736 | tf_op jit(solution)/shard_map/ppermute | solution.py:156
  103.1 25.7 %collective-permute-start.5 = (bf16[1024,512]{1,0:T(8,128)(2,1)}, bf16[1024,512]{1,0:T(8,128)(2,1)}, u32[]{:S(2)}, u32[]{:S(2)}) collective-permute-start(bf16[1024,512]{1,0:T(8,128)(2,1)} %add_convert_fusion.1), channel_id=1, source_target_pairs={{0,2},{1,3},{2,0},{3,1},{4,6},{5,7},{6,4},{7,5},{8,10},{9,11},{10,... | collective-permute-start | bytes 3145736 | tf_op jit(solution)/shard_map/ppermute | solution.py:156
  131.9 29.1 %all-to-all-start.1 = ((bf16[8,128,512]{2,1,0:T(8,128)(2,1)}), bf16[8,128,512]{2,1,0:T(8,128)(2,1)S(1)}, u32[]{:S(2)}, u32[]{:S(2)}) async-start(bf16[8,128,512]{2,1,0:T(8,128)(2,1)} %bitcast.33), calls=%async_computation.2 | async-start | bytes 2097152 | tf_op jit(solution)/shard_map/all_to_all | solution.py:191
  135.6 28.3 %reduce-scatter.2.cloned.1.call-start = ((), (), s32[]{:S(2)}) async-start(), calls=%async_computation.4 | async-start | bytes 655360 | tf_op jit(solution)/shard_map/reduce_scatter | solution.py:115
  139.7 1.4 copy-start.8
Sparse Core Ops, SparseCore 0:
  30.8 48.3 all-gather.1
  141.1 22.7 reduce-scatter.1
